TPU v7x, 256 devices: a whole 4x4x8 slice. The times are simulated.
256 devices in a mesh: ra: 32 (over z, y), cb: 8 (over x, core).
Axes of the slice: x: 4, y: 4, z: 8, core: 2. Of those that a mesh axis runs over, the one named last changes fastest.
Arguments:
- stream: bfloat16 [64, 1024], P(None, 'ra'), may hold values from -24 to 24, as said below
- gain_first: float32 [1024], P('ra'), may hold values from 0.5 to 1.5
- up_first: float32 [1024, 4096], P('ra', 'cb'), may hold values from -0.1875 to 0.1875
- down_first: float32 [4096, 1024], P('cb', 'ra'), may hold values from -0.09375 to 0.09375
- gain_second: float32 [1024], P('ra'), may hold values from 0.5 to 1.5
- up_second: float32 [1024, 4096], P('ra', 'cb'), may hold values from -0.1875 to 0.1875
- down_second: float32 [4096, 1024], P('cb', 'ra'), may hold values from -0.09375 to 0.09375
Outputs:
- read: bfloat16 [64, 1024], P(None, 'ra')
Inputs may be any that keep to these rules, and one draw needn't show every extreme that they name: stream is of order one, and in each token one aligned block of 32 features is four times larger than the rest.
All inputs are finite; a program needn't handle non-finite values.
Results may differ from a plain program's by a relative error of at most 0.025.
Values may be sent and summed in bfloat16 or wider, within the bound.
A program may use at most 64 MiB of HBM per device.

v0:
```python
import jax
import jax.numpy as jnp
from jax import lax
from jax.sharding import Mesh
from jax.sharding import PartitionSpec as P

D = 1024
RA = ("ra_0", "ra_1")
EPS = 1e-06
RESIDUAL = 0.25


def by_axis(array, axes):
    for axis in axes:
        array = lax.psum(array, axis)
    return array


def total_of_pieces(array, axis):
    pieces = lax.all_gather(array, axis)
    return pieces.sum(axis=0)


def over_pieces(array, axis):
    return lax.all_gather(array, axis).astype(jnp.float32).sum(0)


def sublayer(stream, norm_gain, w_up, w_down):
    floated = stream.astype(jnp.float32)
    own_squares = jnp.sum(floated * floated, axis=1, keepdims=True)
    squares = by_axis(own_squares, RA)
    factor = lax.rsqrt(squares / D + EPS)
    normed = (floated * factor * norm_gain.astype(jnp.float32)[None, :]).astype(jnp.bfloat16)
    up_bf = w_up.astype(jnp.bfloat16)
    down_bf = w_down.astype(jnp.bfloat16)
    partial_value = jnp.dot(normed, up_bf, preferred_element_type=jnp.float32)
    preact = total_of_pieces(partial_value, RA)
    activated = jnp.square(jax.nn.relu(preact)).astype(jnp.bfloat16)
    down_part = jnp.dot(activated, down_bf, preferred_element_type=jnp.float32)
    branch = over_pieces(down_part.astype(jnp.bfloat16), "cb").astype(jnp.float32)
    return (RESIDUAL * floated + branch).astype(jnp.bfloat16)


def local(stream, gain_first, up_first, down_first, gain_second, up_second, down_second):
    middle = sublayer(stream, gain_first, up_first, down_first)
    return sublayer(middle, gain_second, up_second, down_second)


def solution(mesh):
    torus = Mesh(mesh.devices.reshape(8, 4, mesh.shape["cb"]), ("ra_0", "ra_1", "cb"))
    in_specs = (P(None, RA), P(RA), P(RA, "cb"), P("cb", RA), P(RA), P(RA, "cb"), P("cb", RA))
    out_specs = P(None, RA)
    return jax.shard_map(local, mesh=torus, in_specs=in_specs, out_specs=out_specs, check_vma=False)
```

profile of v0, /device:TPU:1, one launch (start us, length us, event | category | flops | bytes accessed | tf_op | source)
XLA Modules:
  0.0 262.2 jit_solution(6546073855465038196)
XLA Ops:
  6.5 0.0 all-gather.9.cloned.1.call-start
  6.6 0.8 fusion.12
  7.3 17.3 %psum.28 = f32[64,1]{0,1:T(1,128)S(1)} all-reduce(f32[64,1]{0,1:T(1,128)S(1)} %bitcast.15), channel_id=1, replica_groups=mesh['ra_0'=8,'ra_1'=4,'cb'=8] {'ra_0'}, use_global_device_ids=true, to_apply=%region_1.0 | all-reduce | flops 64 | bytes 512 | tf_op jit(solution)/shard_map/psum | solution.py:15
  24.6 8.7 %psum.29 = f32[64,1]{0,1:T(1,128)S(1)} all-reduce(f32[64,1]{0,1:T(1,128)S(1)} %psum.28), channel_id=1, replica_groups=mesh['ra_0'=8,'ra_1'=4,'cb'=8] {'ra_1'}, use_global_device_ids=true, to_apply=%region_2.0 | all-reduce | flops 64 | bytes 512 | tf_op jit(solution)/shard_map/psum | solution.py:15
  33.3 1.8 fusion.8
  35.1 0.0 all-gather.9.cloned.1.call-update
  35.1 0.0 all-gather.11.cloned.1.call-start
  35.2 79.7 %all-gather.9.cloned.1.call-done = f32[2048,512]{1,0:T(8,128)} async-done(((f32[64,512]{1,0:T(8,128)}), f32[2048,512]{1,0:T(8,128)}) %all-gather.9.cloned.1.call-update) | async-done | bytes 4194320 | tf_op jit(solution)/shard_map/all_gather | solution.py:20
  114.9 2.6 reduce_sum.55
  117.5 0.0 copy-done.1
  117.5 0.1 fusion
  117.6 17.1 %all-gather.4 = bf16[8,64,32]{1,2,0:T(8,128)(2,1)S(1)} all-gather(bf16[1,64,32]{1,2,0:T(8,128)(2,1)S(1)} %fusion), channel_id=3, replica_groups=mesh['ra_0'=8,'ra_1'=4,'cb'=8] {'cb'}, dimensions={0}, use_global_device_ids=true | all-gather | bytes 36864 | tf_op jit(solution)/shard_map/all_gather | solution.py:25
  134.7 0.0 copy-done
  134.8 12.3 %psum.30 = f32[64,1]{0,1:T(1,128)S(1)} all-reduce(f32[64,1]{0,1:T(1,128)S(1)} %bitcast.14), channel_id=1, replica_groups=mesh['ra_0'=8,'ra_1'=4,'cb'=8] {'ra_0'}, use_global_device_ids=true, to_apply=%region_6.7 | all-reduce | flops 64 | bytes 512 | tf_op jit(solution)/shard_map/psum | solution.py:15
  147.1 6.5 %psum.31 = f32[64,1]{0,1:T(1,128)S(1)} all-reduce(f32[64,1]{0,1:T(1,128)S(1)} %psum.30), channel_id=1, replica_groups=mesh['ra_0'=8,'ra_1'=4,'cb'=8] {'ra_1'}, use_global_device_ids=true, to_apply=%region_7.8 | all-reduce | flops 64 | bytes 512 | tf_op jit(solution)/shard_map/psum | solution.py:15
  153.6 0.0 copy-done.2
  153.7 0.0 copy-done.4
  153.7 0.9 fusion.5
  154.6 0.0 all-gather.11.cloned.1.call-update
  154.6 80.4 %all-gather.11.cloned.1.call-done = f32[2048,512]{1,0:T(8,128)} async-done(((f32[64,512]{1,0:T(8,128)}), f32[2048,512]{1,0:T(8,128)}) %all-gather.11.cloned.1.call-update) | async-done | bytes 4194320 | tf_op jit(solution)/shard_map/all_gather | solution.py:20
  234.9 2.5 reduce_sum.58
  237.5 0.1 fusion.1
  237.6 17.1 %all-gather.5 = bf16[8,64,32]{1,2,0:T(8,128)(2,1)S(1)} all-gather(bf16[1,64,32]{1,2,0:T(8,128)(2,1)S(1)} %fusion.1), channel_id=5, replica_groups=mesh['ra_0'=8,'ra_1'=4,'cb'=8] {'cb'}, dimensions={0}, use_global_device_ids=true | all-gather | bytes 36864 | tf_op jit(solution)/shard_map/all_gather | solution.py:25
  254.7 0.6 fusion.16
  (11 shorter events, 0.1 us)
Async XLA Ops:
  6.5 128.2 %copy-start = (bf16[64,32]{0,1:T(8,128)(2,1)S(1)}, bf16[64,32]{0,1:T(8,128)(2,1)}, u32[]{:S(2)}) copy-start(bf16[64,32]{0,1:T(8,128)(2,1)} %param.7) | copy-start | bytes 12292
  6.5 111.0 %copy-start.1 = (f32[512,32]{0,1:T(8,128)S(1)}, f32[512,32]{0,1:T(8,128)}, u32[]{:S(2)}) copy-start(f32[512,32]{0,1:T(8,128)} %param.10) | copy-start | bytes 196612
  6.5 147.1 %copy-start.2 = (f32[32,512]{1,0:T(8,128)S(1)}, f32[32,512]{1,0:T(8,128)}, u32[]{:S(2)}) copy-start(f32[32,512]{1,0:T(8,128)} %param.12) | copy-start | bytes 196612
  6.5 147.1 %copy-start.4 = (f32[32]{0:T(128)S(1)}, f32[32]{0:T(128)}, u32[]{:S(2)}) copy-start(f32[32]{0:T(128)} %param.11) | copy-start | bytes 388
  6.5 108.4 %all-gather.9.cloned.1.call-start = ((), (), s32[]{:S(2)}) async-start(), calls=%async_computation | async-start | bytes 4325376 | tf_op jit(solution)/shard_map/all_gather | solution.py:20
  35.1 199.8 %all-gather.11.cloned.1.call-start = ((), (), s32[]{:S(2)}) async-start(), calls=%async_computation.1 | async-start | bytes 4325376 | tf_op jit(solution)/shard_map/all_gather | solution.py:20
  114.9 122.5 %copy-start.3 = (f32[512,32]{0,1:T(8,128)S(1)}, f32[512,32]{0,1:T(8,128)}, u32[]{:S(2)}) copy-start(f32[512,32]{0,1:T(8,128)} %param.13) | copy-start | bytes 196612
Sparse Core Ops, SparseCore 0:
  35.3 79.6 all-gather.8
  154.7 80.1 all-gather.10
where the time goes:
time: 262 us
  waiting for transfers between devices  160 us (61%)
  blocking collectives  79 us (30%)
  between operations  13.4 us (5%)
  other arithmetic  6.52 us (2%)
  matrix products  2.95 us (1%)
    all_gather x2, waiting for transfers between devices, total_of_pieces(): pieces = lax.all_gather(array, axis)  160 us
    psum x4, blocking collectives, by_axis(): array = lax.psum(array, axis)  44.9 us
    all_gather x2, blocking collectives, over_pieces(): return lax.all_gather(array, axis).astype(jnp.float32).sum(0)  34.2 us
  transfers between devices with their start and end apart: 2, of which 2 were waited for; matrix products, arithmetic and copies ran while one was open for 0% of the time, Pallas kernels for 0%

commit v1 on v0

--- a/solution.py
+++ b/solution.py
@@ -12,7 +12,7 @@
 
 def by_axis(array, axes):
     for axis in axes:
-        array = lax.psum(array, axis)
+        array = jnp.sum(lax.all_gather(array, axis), axis=0)
     return array
 
 

time: 262 us -> 268 us (1.023)
  local copies, waits for them, and re-layouts: 0.02 us -> 3.88 us
    psum x4 -> x0, blocking collectives: 44.9 us -> none  [by_axis(): array = lax.psum(array, axis)]
    unnamed x0 -> x4, blocking collectives: none -> 44.8 us
    unnamed x10 -> x20, local copies, waits for them, and re-layouts: 0.02 us -> 3.55 us
where the time goes in v1:
time: 268 us; the launch traced here: 267 us
  waiting for transfers between devices  160 us (60%)
  blocking collectives  79 us (29%)
  between operations  14.8 us (6%)
  other arithmetic  6.61 us (2%)
  local copies, waits for them, and re-layouts  3.88 us (1%)
  matrix products  2.95 us (1%)
    all_gather x2, waiting for transfers between devices, total_of_pieces(): pieces = lax.all_gather(array, axis)  160 us
    unnamed x4, blocking collectives  44.8 us
    all_gather x2, blocking collectives, over_pieces(): return lax.all_gather(array, axis).astype(jnp.float32).sum(0)  34.2 us
  transfers between devices with their start and end apart: 2, of which 2 were waited for; matrix products, arithmetic and copies ran while one was open for 0% of the time, Pallas kernels for 0%

profile of v1, /device:TPU:1, one launch (start us, length us, event | category | flops | bytes accessed | tf_op | source)
XLA Modules:
  0.0 267.4 jit_solution(8511208917221614598)
XLA Ops:
  6.6 0.8 fusion.12
  7.3 1.3 dynamic-slice
  9.3 0.2 dynamic-update-slice
  9.5 17.3 %all-reduce = f32[512]{0:T(512)S(1)} all-reduce(f32[512]{0:T(512)S(1)} %dynamic-update-slice), channel_id=2, replica_groups=mesh['ra_0'=8,'ra_1'=4,'cb'=8] {'ra_0'}, use_global_device_ids=true, to_apply=%add | all-reduce | flops 512 | bytes 4096
  26.9 1.3 dynamic-slice.1
  28.8 0.2 dynamic-update-slice.1
  29.0 8.7 %all-reduce.1 = f32[256]{0:T(256)S(1)} all-reduce(f32[256]{0:T(256)S(1)} %dynamic-update-slice.1), channel_id=3, replica_groups=mesh['ra_0'=8,'ra_1'=4,'cb'=8] {'ra_1'}, use_global_device_ids=true, to_apply=%add.1 | all-reduce | flops 256 | bytes 2048
  37.7 0.1 reshape.25
  37.9 1.8 fusion.8
  39.7 79.7 %all-gather.13.cloned.1.call-done = f32[2048,512]{1,0:T(8,128)} async-done(((f32[64,512]{1,0:T(8,128)}), f32[2048,512]{1,0:T(8,128)}) %all-gather.13.cloned.1.call-update) | async-done | bytes 4194320 | tf_op jit(solution)/shard_map/all_gather | solution.py:20
  119.4 2.6 reduce_sum.93
  122.0 0.1 fusion
  122.1 17.1 %all-gather.8 = bf16[8,64,32]{1,2,0:T(8,128)(2,1)S(1)} all-gather(bf16[1,64,32]{1,2,0:T(8,128)(2,1)S(1)} %fusion), channel_id=5, replica_groups=mesh['ra_0'=8,'ra_1'=4,'cb'=8] {'cb'}, dimensions={0}, use_global_device_ids=true | all-gather | bytes 36864 | tf_op jit(solution)/shard_map/all_gather | solution.py:25
  139.3 0.2 dynamic-update-slice.2
  139.5 12.3 %all-reduce.2 = f32[512]{0:T(512)S(1)} all-reduce(f32[512]{0:T(512)S(1)} %dynamic-update-slice.2), channel_id=6, replica_groups=mesh['ra_0'=8,'ra_1'=4,'cb'=8] {'ra_0'}, use_global_device_ids=true, to_apply=%add.2 | all-reduce | flops 512 | bytes 4096
  152.0 0.2 dynamic-update-slice.3
  152.2 6.5 %all-reduce.3 = f32[256]{0:T(256)S(1)} all-reduce(f32[256]{0:T(256)S(1)} %dynamic-update-slice.3), channel_id=7, replica_groups=mesh['ra_0'=8,'ra_1'=4,'cb'=8] {'ra_1'}, use_global_device_ids=true, to_apply=%add.3 | all-reduce | flops 256 | bytes 2048
  158.7 0.1 reshape.29
  158.8 0.9 fusion.5
  159.8 80.4 %all-gather.15.cloned.1.call-done = f32[2048,512]{1,0:T(8,128)} async-done(((f32[64,512]{1,0:T(8,128)}), f32[2048,512]{1,0:T(8,128)}) %all-gather.15.cloned.1.call-update) | async-done | bytes 4194320 | tf_op jit(solution)/shard_map/all_gather | solution.py:20
  240.1 2.5 reduce_sum.98
  242.7 0.1 fusion.1
  242.8 17.1 %all-gather.9 = bf16[8,64,32]{1,2,0:T(8,128)(2,1)S(1)} all-gather(bf16[1,64,32]{1,2,0:T(8,128)(2,1)S(1)} %fusion.1), channel_id=9, replica_groups=mesh['ra_0'=8,'ra_1'=4,'cb'=8] {'cb'}, dimensions={0}, use_global_device_ids=true | all-gather | bytes 36864 | tf_op jit(solution)/shard_map/all_gather | solution.py:25
  259.9 0.6 fusion.16
  (29 shorter events, 0.5 us)
Async XLA Ops:
  6.5 132.7 %copy-start = (bf16[64,32]{0,1:T(8,128)(2,1)S(1)}, bf16[64,32]{0,1:T(8,128)(2,1)}, u32[]{:S(2)}) copy-start(bf16[64,32]{0,1:T(8,128)(2,1)} %param.7) | copy-start | bytes 12292
  6.5 115.5 %copy-start.1 = (f32[512,32]{0,1:T(8,128)S(1)}, f32[512,32]{0,1:T(8,128)}, u32[]{:S(2)}) copy-start(f32[512,32]{0,1:T(8,128)} %param.10) | copy-start | bytes 196612
  6.5 152.3 %copy-start.4 = (f32[32]{0:T(128)S(1)}, f32[32]{0:T(128)}, u32[]{:S(2)}) copy-start(f32[32]{0:T(128)} %param.11) | copy-start | bytes 388
  6.5 152.3 %copy-start.2 = (f32[32,512]{1,0:T(8,128)S(1)}, f32[32,512]{1,0:T(8,128)}, u32[]{:S(2)}) copy-start(f32[32,512]{1,0:T(8,128)} %param.12) | copy-start | bytes 196612
  6.5 112.9 %all-gather.13.cloned.1.call-start = ((), (), s32[]{:S(2)}) async-start(), calls=%async_computation | async-start | bytes 4325376 | tf_op jit(solution)/shard_map/all_gather | solution.py:20
  39.7 200.5 %all-gather.15.cloned.1.call-start = ((), (), s32[]{:S(2)}) async-start(), calls=%async_computation.1 | async-start | bytes 4325376 | tf_op jit(solution)/shard_map/all_gather | solution.py:20
  119.4 123.2 %copy-start.3 = (f32[512,32]{0,1:T(8,128)S(1)}, f32[512,32]{0,1:T(8,128)}, u32[]{:S(2)}) copy-start(f32[512,32]{0,1:T(8,128)} %param.13) | copy-start | bytes 196612
Sparse Core Ops, SparseCore 0:
  39.8 79.6 all-gather.12
  159.9 80.1 all-gather.14
